TPU v7x, 512 devices: a 8x2x16 block of a 8x16x16 slice. The times are simulated.
512 devices in a mesh: grp: 2 (over y), sp: 16 (over z), tp: 16 (over x, core).
Axes of the slice: x: 8, y: 2, z: 16, core: 2. Of those that a mesh axis runs over, the one named last changes fastest.
The devices are a block of a 8x16x16 slice.
Arguments:
- target: bfloat16 [4096, 2048], P(('grp', 'sp', 'tp')), parts along dimension 0, may hold values from -6 to 6
- source: bfloat16 [32768, 2048], P(('grp', 'sp', 'tp')), parts along dimension 0, may hold values from -6 to 6
- norm_gain: float32 [2048], replicated, may hold values from 0.1 to 1.9
- query_weight: bfloat16 [2048, 2048], P(None, 'tp'), may hold values from -0.125 to 0.125
- key_weight: bfloat16 [2048, 256], replicated, may hold values from -0.125 to 0.125
- value_weight: bfloat16 [2048, 256], replicated, may hold values from -0.125 to 0.125
- output_weight: bfloat16 [2048, 2048], P('tp'), may hold values from -0.125 to 0.125
- saved_out: bfloat16 [4096, 2048], P(('grp', 'sp'), 'tp'), parts along dimension 0, may hold values from -3 to 3
- log_shift: float32 [16, 4096], P('tp', ('grp', 'sp')), parts along dimension 1, may hold values from 0 to 2
- out_grad: bfloat16 [4096, 2048], P(('grp', 'sp', 'tp')), parts along dimension 0, may hold values from -48 to 48
Outputs:
- target_grad: float32 [4096, 2048], P(('grp', 'sp', 'tp')), parts along dimension 0
- source_grad: float32 [32768, 2048], P(('grp', 'sp', 'tp')), parts along dimension 0
- query_weight_grad: float32 [4096, 2048], P(('grp', 'sp'), 'tp'), parts along dimension 0
There are 2 independent parts, one for each index of `grp`. A program takes and returns all parts, laid end to end along the dimension named above; an argument that names none is the same for every part. Nothing has to cross between parts.
All inputs are finite; a program needn't handle non-finite values.
Results may differ from a plain program's by a relative error of at most 0.02.
Values may be sent and summed in bfloat16 or wider, within the bound.
A program may use at most 64 MiB of HBM per device.

v0:
```python
import jax
import jax.numpy as jnp
from jax import lax
from jax.sharding import PartitionSpec as P

HEADS = 16
HEAD_DIM = 128
KV_HEADS = 2


def cut_along(array, dim, count):
    dims = array.shape
    blocks = array.reshape(*dims[:dim], count, dims[dim] // count, *dims[dim + 1 :])
    return jnp.moveaxis(blocks, dim, 0)


def summed_on_arrival(array, axis, dim):
    blocks = cut_along(array, dim, lax.axis_size(axis))
    arrived = lax.all_to_all(blocks, axis, split_axis=0, concat_axis=0, tiled=True)
    return arrived.astype(jnp.float32).sum(axis=0)


def attend(query_heads, back_heads, shift_cols, drop_cols, key_rows, values, offset):
    factor = HEAD_DIM ** (-0.5)
    scores = (
        jnp.einsum("nhd,md->hnm", query_heads, key_rows, preferred_element_type=jnp.float32)
        * factor
    )
    prob = jnp.exp(scores - shift_cols.T[:, :, None] - offset)
    prob_grad = jnp.einsum("nhd,md->hnm", back_heads, values, preferred_element_type=jnp.float32)
    score_grad = (prob * (prob_grad - drop_cols.T[:, :, None]) * factor).astype(jnp.bfloat16)
    return (prob.astype(jnp.bfloat16), score_grad)


def shards(
    target,
    source,
    norm_gain,
    query_weight,
    key_weight,
    value_weight,
    output_weight,
    saved_out,
    log_shift,
    out_grad,
):
    tp_count = lax.axis_size("tp")
    sp_count = lax.axis_size("sp")
    local_heads = query_weight.shape[1] // HEAD_DIM
    head_width = local_heads * HEAD_DIM
    model_width = target.shape[1]
    group_size = HEADS // KV_HEADS
    pair_index = lax.axis_index("tp") * local_heads // group_size
    offset = jnp.log(jnp.float32(source.shape[0] * tp_count * sp_count))
    target_wide = target.astype(jnp.float32)
    root_mean = jnp.sqrt(jnp.mean(target_wide * target_wide, axis=1, keepdims=True) + 1e-06)
    normed = (target_wide / root_mean * norm_gain).astype(jnp.bfloat16)
    joined = jnp.concatenate([normed, out_grad], axis=1)
    portion = lax.all_gather(joined, "tp", axis=0, tiled=True)
    normed_part = portion[:, :model_width]
    query_part = jnp.dot(normed_part, query_weight, preferred_element_type=jnp.float32).astype(
        jnp.bfloat16
    )
    back_part = lax.dot_general(
        portion[:, model_width:],
        output_weight,
        (((1,), (1,)), ((), ())),
        preferred_element_type=jnp.float32,
    ).astype(jnp.bfloat16)
    gathered = jnp.concatenate([query_part, back_part, normed_part], axis=1)
    queries = gathered[:, :head_width]
    out_back = gathered[:, head_width : 2 * head_width]
    normed_all = gathered[:, 2 * head_width :]
    tgt_local = queries.shape[0]
    key_cols = lax.dynamic_slice_in_dim(key_weight, pair_index * HEAD_DIM, HEAD_DIM, 1)
    value_cols = lax.dynamic_slice_in_dim(value_weight, pair_index * HEAD_DIM, HEAD_DIM, 1)
    both_cols = jnp.concatenate([key_cols, value_cols], axis=1)
    paired = jnp.dot(
        lax.all_gather(source, "tp", axis=0, tiled=True),
        both_cols,
        preferred_element_type=jnp.float32,
    ).astype(jnp.bfloat16)
    key_rows = paired[:, :HEAD_DIM]
    values = paired[:, HEAD_DIM:]
    products = out_back.astype(jnp.float32) * saved_out.astype(jnp.float32)
    drop_cols = jnp.sum(products.reshape(tgt_local, local_heads, HEAD_DIM), axis=2)
    shift_cols = log_shift.T
    portion = (
        lax.all_gather(queries, "sp", axis=0, tiled=True),
        lax.all_gather(out_back, "sp", axis=0, tiled=True),
        lax.all_gather(shift_cols.astype(jnp.bfloat16), "sp", axis=0, tiled=True).astype(
            jnp.float32
        ),
        lax.all_gather(drop_cols.astype(jnp.bfloat16), "sp", axis=0, tiled=True).astype(
            jnp.float32
        ),
    )
    query_part, back_part, shift_part, drop_part = portion
    count_rows = query_part.shape[0]
    query_three = query_part.reshape(count_rows, local_heads, HEAD_DIM)
    back_three = back_part.reshape(count_rows, local_heads, HEAD_DIM)
    prob_low, score_grad = attend(
        query_three, back_three, shift_part, drop_part, key_rows, values, offset
    )
    key_sum = jnp.einsum("hnm,nhd->md", score_grad, query_three, preferred_element_type=jnp.float32)
    value_sum = jnp.einsum("hnm,nhd->md", prob_low, back_three, preferred_element_type=jnp.float32)
    key_sum, value_sum, score_grad = (key_sum, value_sum, score_grad)
    count_rows = portion[0].shape[0]
    added = jnp.einsum(
        "hnm,md->nhd", score_grad, key_rows, preferred_element_type=jnp.float32
    ).reshape(count_rows, head_width)
    query_sum = summed_on_arrival(added.astype(jnp.bfloat16), "sp", 0)
    query_grad = query_sum.astype(jnp.bfloat16)
    stacked = jnp.concatenate([key_sum, value_sum], axis=1)[:, None, :]
    received = lax.all_to_all(
        stacked.astype(jnp.bfloat16), "tp", split_axis=0, concat_axis=1, tiled=True
    ).astype(stacked.dtype)
    own_rows = received.shape[0]
    grouped = jnp.sum(
        received.reshape(own_rows, KV_HEADS, tp_count // KV_HEADS, 2 * HEAD_DIM), axis=2
    )
    key_grad = grouped[:, :, :HEAD_DIM].reshape(own_rows, KV_HEADS * HEAD_DIM).astype(jnp.bfloat16)
    value_grad = (
        grouped[:, :, HEAD_DIM:].reshape(own_rows, KV_HEADS * HEAD_DIM).astype(jnp.bfloat16)
    )
    contract = (((1,), (1,)), ((), ()))
    source_grad = lax.dot_general(
        key_grad, key_weight, contract, preferred_element_type=jnp.float32
    ) + lax.dot_general(value_grad, value_weight, contract, preferred_element_type=jnp.float32)
    picked = query_grad
    normed_grad = summed_on_arrival(
        lax.dot_general(picked, query_weight, contract, preferred_element_type=jnp.float32).astype(
            jnp.bfloat16
        ),
        "tp",
        0,
    )
    scaled_grad = normed_grad * norm_gain
    target_grad = (
        scaled_grad / root_mean
        - target_wide * jnp.mean(scaled_grad * target_wide, axis=1, keepdims=True) / root_mean**3
    )
    picked = normed_all
    query_weight_grad = summed_on_arrival(
        lax.dot_general(
            picked, query_grad, (((0,), (0,)), ((), ())), preferred_element_type=jnp.float32
        ).astype(jnp.bfloat16),
        "sp",
        0,
    )
    return (target_grad, source_grad, query_weight_grad)


def solution(mesh):
    return jax.shard_map(
        shards,
        mesh=mesh,
        in_specs=(
            P(("grp", "sp", "tp"), None),
            P(("grp", "sp", "tp"), None),
            P(),
            P(None, "tp"),
            P(),
            P(),
            P("tp", None),
            P(("grp", "sp"), "tp"),
            P("tp", ("grp", "sp")),
            P(("grp", "sp", "tp"), None),
        ),
        out_specs=(
            P(("grp", "sp", "tp"), None),
            P(("grp", "sp", "tp"), None),
            P(("grp", "sp"), "tp"),
        ),
        check_vma=False,
    )
```

profile of v0, /device:TPU:80, one launch (start us, length us, event | category | flops | bytes accessed | tf_op | source)
XLA Modules:
  0.0 304.8 jit_solution(2163993728256108957)
XLA Ops:
  7.2 0.0 copy-start
  7.2 0.1 all-gather.8.cloned.1.call-start
  7.3 0.9 fusion.43
  8.2 0.8 fusion.45
  9.1 1.4 pad_maximum_fusion.1
  10.4 0.1 all-gather.8.cloned.1.call-update
  10.5 0.1 all-gather.6.cloned.1.call-start
  10.6 0.7 all-gather.6.cloned.1.call-update
  11.3 0.9 copy.20
  12.2 0.7 convert_element_type.126
  12.9 68.0 %all-gather = bf16[1,2048]{1,0:T(2,128)(2,1)S(1)} all-gather(bf16[1,128]{1,0:T(2,128)(2,1)S(1)} %convert_element_type.126), channel_id=2, replica_groups=mesh['grp'=2,'sp'=16,'tp'=16] {'sp'}, dimensions={1}, use_global_device_ids=true | all-gather | bytes 4352 | tf_op jit(solution)/shard_map/all_gather | solution.py:91
  80.9 1.3 constant_dynamic-slice_fusion
  82.2 5.7 %all-gather.8.cloned.1.call-done = bf16[128,4096]{1,0:T(8,128)(2,1)} async-done(((bf16[8,4096]{1,0:T(8,128)(2,1)}), bf16[128,4096]{1,0:T(8,128)(2,1)}) %all-gather.8.cloned.1.call-update) | async-done | bytes 1048592 | tf_op jit(solution)/shard_map/all_gather | solution.py:59
  87.9 1.5 multiply_reduce_fusion
  89.5 31.1 %all-gather.2 = bf16[16,1,128]{2,1,0:T(2,128)(2,1)S(1)} all-gather(bf16[1,1,128]{2,1,0:T(2,128)(2,1)S(1)} %bitcast.104), channel_id=3, replica_groups=mesh['grp'=2,'sp'=16,'tp'=16] {'sp'}, dimensions={0}, use_global_device_ids=true | all-gather | bytes 4352 | tf_op jit(solution)/shard_map/all_gather | solution.py:94
  120.6 0.0 copy-done
  120.6 1.3 convolution_convert_fusion.4
  121.9 30.0 %all_gather.20 = bf16[2048,128]{1,0:T(8,128)(2,1)S(1)} all-gather(bf16[128,128]{1,0:T(8,128)(2,1)S(1)} %convolution_convert_fusion.4), channel_id=1, replica_groups=mesh['grp'=2,'sp'=16,'tp'=16] {'sp'}, dimensions={0}, use_global_device_ids=true | all-gather | bytes 557056 | tf_op jit(solution)/shard_map/all_gather | solution.py:89
  151.9 31.3 %all_gather.22 = bf16[2048,128]{0,1:T(8,128)(2,1)S(1)} all-gather(bf16[128,128]{0,1:T(8,128)(2,1)S(1)} %get-tuple-element.8), channel_id=1, replica_groups=mesh['grp'=2,'sp'=16,'tp'=16] {'sp'}, dimensions={0}, use_global_device_ids=true | all-gather | bytes 557056 | tf_op jit(solution)/shard_map/all_gather | solution.py:90
  183.2 0.0 all-gather.6.cloned.1.call-done
  183.2 3.5 %fusion.17 = bf16[1024,256]{0,1:T(8,128)(2,1)S(1)} fusion(bf16[1024,2048]{1,0:T(8,128)(2,1)} %all-gather.6.cloned.1.call-done, bf16[2048,128]{1,0:T(8,128)(2,1)S(1)} %get-tuple-element.9, bf16[2048,128]{1,0:T(8,128)(2,1)S(1)} %get-tuple-element.10), kind=kOutput, calls=%fused_computation.20 | convolution fusion | flops 1076101120 | bytes 5767168 | tf_op jit(solution)/shard_map/dot_general | solution.py:78
  186.7 1.3 fusion.41
  188.0 0.0 copy-start.1
  188.0 2.9 fusion.2
  191.0 0.0 copy-start.2
  191.0 0.7 fusion.18
  191.7 0.0 copy-done.1
  191.7 0.1 copy.30
  191.8 1.1 copy-done.2
  192.9 0.9 copy.21
  193.8 7.6 %all-to-all-start = ((bf16[16,128,128]{1,2,0:T(8,128)(2,1)}), bf16[16,128,128]{1,2,0:T(8,128)(2,1)S(1)}, u32[]{:S(2)}, u32[]{:S(2)}) async-start(bf16[16,128,128]{1,2,0:T(8,128)(2,1)} %copy.21), calls=%async_computation | async-start | bytes 1048576 | tf_op jit(solution)/shard_map/all_to_all | solution.py:19
  201.4 3.7 %fusion.27 = bf16[1024,1,128]{0,2,1:T(8,128)(2,1)S(1)} fusion(bf16[2048,128]{1,0:T(8,128)(2,1)S(1)} %all_gather.20, bf16[1024,2048,1]{1,0,2:T(8,128)(2,1)} %copy-done.2), kind=kOutput, calls=%fused_computation.24 | convolution fusion | flops 537001984 | bytes 4980736 | tf_op jit(solution)/shard_map/hnm,nhd->md/dot_general | solution.py:105
  205.1 5.3 %fusion.30 = bf16[1024,1,128]{0,2,1:T(8,128)(2,1)S(1)} fusion(bf16[2048,128]{0,1:T(8,128)(2,1)S(1)} %all_gather.22, f32[1024,2048]{1,0:T(8,128)} %copy-done.1, f32[2048]{0:T(1024)S(1)} %bitcast.102), kind=kOutput, calls=%fused_computation.25 | convolution fusion | flops 545390592 | bytes 9183232 | tf_op jit(solution)/shard_map/hnm,nhd->md/dot_general | solution.py:106
  210.5 0.0 copy-start.3
  210.5 0.5 broadcast.79
  211.0 0.0 copy-start.5
  211.0 0.0 copy-start.6
  211.0 1.0 reduce.4
  212.1 0.2 copy.39
  212.3 0.9 reshape.147
  213.2 6.6 %all-to-all-done = bf16[16,128,128]{1,2,0:T(8,128)(2,1)S(1)} async-done(((bf16[16,128,128]{1,2,0:T(8,128)(2,1)}), bf16[16,128,128]{1,2,0:T(8,128)(2,1)S(1)}, u32[]{:S(2)}, u32[]{:S(2)}) %all-to-all-start) | async-done | bytes 524320 | tf_op jit(solution)/shard_map/all_to_all | solution.py:19
  219.8 4.7 %all-to-all-start.2 = ((bf16[16,2,8192]{2,1,0:T(2,128)(2,1)}), bf16[16,2,8192]{2,1,0:T(2,128)(2,1)S(1)}, u32[]{:S(2)}, u32[]{:S(2)}) async-start(bf16[16,2,8192]{2,1,0:T(2,128)(2,1)} %reshape.147), calls=%async_computation.2 | async-start | bytes 1048576 | tf_op jit(solution)/shard_map/all_to_all | solution.py:115
  224.5 0.1 reduce_sum.68
  224.6 1.1 fusion.16
  225.7 14.5 %all-to-all-done.2 = bf16[16,2,8192]{2,1,0:T(2,128)(2,1)S(1)} async-done(((bf16[16,2,8192]{2,1,0:T(2,128)(2,1)}), bf16[16,2,8192]{2,1,0:T(2,128)(2,1)S(1)}, u32[]{:S(2)}, u32[]{:S(2)}) %all-to-all-start.2) | async-done | bytes 524320 | tf_op jit(solution)/shard_map/all_to_all | solution.py:115
  240.2 4.5 %all-to-all-start.1 = ((bf16[16,8,2048]{2,1,0:T(8,128)(2,1)}), bf16[16,8,2048]{2,1,0:T(8,128)(2,1)S(1)}, u32[]{:S(2)}, u32[]{:S(2)}) async-start(bf16[16,8,2048]{2,1,0:T(8,128)(2,1)} %fusion.16), calls=%async_computation.1 | async-start | bytes 1048576 | tf_op jit(solution)/shard_map/all_to_all | solution.py:19
  244.7 2.2 convolution_convert_fusion
  246.9 13.8 %all-to-all-done.1 = bf16[16,8,2048]{2,1,0:T(8,128)(2,1)S(1)} async-done(((bf16[16,8,2048]{2,1,0:T(8,128)(2,1)}), bf16[16,8,2048]{2,1,0:T(8,128)(2,1)S(1)}, u32[]{:S(2)}, u32[]{:S(2)}) %all-to-all-start.1) | async-done | bytes 524320 | tf_op jit(solution)/shard_map/all_to_all | solution.py:19
  260.6 0.0 copy-start.4
  260.6 0.8 copy-done.4
  261.4 7.2 %all-to-all-start.3 = ((bf16[16,128,128]{2,1,0:T(8,128)(2,1)}), bf16[16,128,128]{2,1,0:T(8,128)(2,1)}, u32[]{:S(2)}, u32[]{:S(2)}) async-start(bf16[16,128,128]{2,1,0:T(8,128)(2,1)} %bitcast.18), calls=%async_computation.3 | async-start | bytes 1048576 | tf_op jit(solution)/shard_map/all_to_all | solution.py:19
  268.6 0.5 reshape.148
  269.2 0.1 copy.26
  269.3 0.1 reduce.3
  269.4 0.0 copy-done.3
  269.4 0.4 fusion.51
  269.8 2.5 convolution_add_fusion
  272.3 1.1 convert_reduce_fusion.1
  273.4 0.0 copy-done.5
  273.4 0.0 copy-done.6
  273.4 0.1 fusion.46
  273.6 0.7 fusion.48
  274.3 21.9 %all-to-all-done.3 = bf16[16,128,128]{2,1,0:T(8,128)(2,1)} async-done(((bf16[16,128,128]{2,1,0:T(8,128)(2,1)}), bf16[16,128,128]{2,1,0:T(8,128)(2,1)}, u32[]{:S(2)}, u32[]{:S(2)}) %all-to-all-start.3) | async-done | bytes 524320 | tf_op jit(solution)/shard_map/all_to_all | solution.py:19
  296.2 1.7 convert_reduce_fusion
  (6 shorter events, 0.1 us)
Async XLA Ops:
  7.2 113.4 %copy-start = (bf16[2048,128]{1,0:T(8,128)(2,1)S(1)}, bf16[2048,128]{1,0:T(8,128)(2,1)}, u32[]{:S(2)}) copy-start(bf16[2048,128]{1,0:T(8,128)(2,1)} %param.13) | copy-start | bytes 1572868
  7.2 80.8 %all-gather.8.cloned.1.call-start = ((), (), s32[]{:S(2)}) async-start(), calls=%async_computation.5 | async-start | bytes 1114112 | tf_op jit(solution)/shard_map/all_gather | solution.py:59
  10.5 172.7 %all-gather.6.cloned.1.call-start = ((), (), s32[]{:S(2)}) async-start(), calls=%async_computation.4 | async-start | bytes 4456448 | tf_op jit(solution)/shard_map/all_gather | solution.py:79
  188.0 3.7 %copy-start.1 = (f32[1024,2048]{1,0:T(8,128)}, f32[1024,2048]{1,0:T(8,128)S(1)}, u32[]{:S(2)}) copy-start(f32[1024,2048]{1,0:T(8,128)S(1)} %fusion.41) | copy-start | bytes 25165828
  191.0 2.0 copy-start.2
  193.8 26.0 %all-to-all-start = ((bf16[16,128,128]{1,2,0:T(8,128)(2,1)}), bf16[16,128,128]{1,2,0:T(8,128)(2,1)S(1)}, u32[]{:S(2)}, u32[]{:S(2)}) async-start(bf16[16,128,128]{1,2,0:T(8,128)(2,1)} %copy.21), calls=%async_computation | async-start | bytes 1048576 | tf_op jit(solution)/shard_map/all_to_all | solution.py:19
  210.5 58.9 %copy-start.3 = (bf16[2048,256]{1,0:T(8,128)(2,1)S(1)}, bf16[2048,256]{1,0:T(8,128)(2,1)}, u32[]{:S(2)}) copy-start(bf16[2048,256]{1,0:T(8,128)(2,1)} %param.14) | copy-start | bytes 3145732
  211.0 62.4 %copy-start.5 = (bf16[8,2048]{1,0:T(8,128)(2,1)S(1)}, bf16[8,2048]{1,0:T(8,128)(2,1)}, u32[]{:S(2)}) copy-start(bf16[8,2048]{1,0:T(8,128)(2,1)} %param.10) | copy-start | bytes 98308
  211.0 62.4 %copy-start.6 = (f32[2048]{0:T(1024)S(1)}, f32[2048]{0:T(1024)}, u32[]{:S(2)}) copy-start(f32[2048]{0:T(1024)} %param.12) | copy-start | bytes 24580
  219.8 20.4 %all-to-all-start.2 = ((bf16[16,2,8192]{2,1,0:T(2,128)(2,1)}), bf16[16,2,8192]{2,1,0:T(2,128)(2,1)S(1)}, u32[]{:S(2)}, u32[]{:S(2)}) async-start(bf16[16,2,8192]{2,1,0:T(2,128)(2,1)} %reshape.147), calls=%async_computation.2 | async-start | bytes 1048576 | tf_op jit(solution)/shard_map/all_to_all | solution.py:115
  240.2 20.4 %all-to-all-start.1 = ((bf16[16,8,2048]{2,1,0:T(8,128)(2,1)}), bf16[16,8,2048]{2,1,0:T(8,128)(2,1)S(1)}, u32[]{:S(2)}, u32[]{:S(2)}) async-start(bf16[16,8,2048]{2,1,0:T(8,128)(2,1)} %fusion.16), calls=%async_computation.1 | async-start | bytes 1048576 | tf_op jit(solution)/shard_map/all_to_all | solution.py:19
  260.6 0.8 copy-start.4
  261.4 34.8 %all-to-all-start.3 = ((bf16[16,128,128]{2,1,0:T(8,128)(2,1)}), bf16[16,128,128]{2,1,0:T(8,128)(2,1)}, u32[]{:S(2)}, u32[]{:S(2)}) async-start(bf16[16,128,128]{2,1,0:T(8,128)(2,1)} %bitcast.18), calls=%async_computation.3 | async-start | bytes 1048576 | tf_op jit(solution)/shard_map/all_to_all | solution.py:19
Sparse Core Ops, SparseCore 0:
  10.7 77.1 all-gather.7
  90.1 47.4 all-gather.5
where the time goes:
time: 310 us; the launch traced here: 305 us
  blocking collectives  160 us (52%)
  waiting for transfers between devices  63.4 us (20%)
  matrix products  26.5 us (9%)
  starting transfers between devices  24 us (8%)
  between operations  14.3 us (5%)
  other arithmetic  8.83 us (3%)
  local copies, waits for them, and re-layouts  7.35 us (2%)
    all_gather x1, blocking collectives, shards(): lax.all_gather(shift_cols.astype(jnp.bfloat16), 'sp', axis=0, tiled=True)  68 us
    all_to_all x3, waiting for transfers between devices, summed_on_arrival(): lax.all_to_all(blocks, axis, split_axis=0, concat_axis=0, tiled=True)  42.3 us
    all_gather x1, blocking collectives, shards(): lax.all_gather(out_back, 'sp', axis=0, tiled=True)  31.3 us
    all_gather x1, blocking collectives, shards(): lax.all_gather(drop_cols.astype(jnp.bfloat16), 'sp', axis=0, tiled=True)  31.1 us
    all_gather x1, blocking collectives, shards(): lax.all_gather(queries, 'sp', axis=0, tiled=True)  30 us
    all_to_all x3, starting transfers between devices, summed_on_arrival(): lax.all_to_all(blocks, axis, split_axis=0, concat_axis=0, tiled=True)  19.2 us
    all_to_all x1, waiting for transfers between devices, shards(): lax.all_to_all(stacked.astype(jnp.bfloat16), 'tp', split_axis=0, concat_a...  14.5 us
  transfers between devices with their start and end apart: 6, of which 5 were waited for; matrix products, arithmetic and copies ran while one was open for 9% of the time, Pallas kernels for 0%

commit v1 on v0

v1 whole, which is shorter than its diff:
```python
import functools
import math

import jax
import jax.numpy as jnp
from jax import lax
from jax.experimental import pallas as pl
from jax.experimental.pallas import tpu as pltpu
from jax.sharding import PartitionSpec as P

HEAD_DIM = 128
KV_HEADS = 2
A_SUBS = 4
C_SUBS = 2
R_SUBS = 2
TILE = 512
FIRST = 3
LOG2E = math.log2(math.e)
F32, BF16 = jnp.float32, jnp.bfloat16
NT = (((1,), (1,)), ((), ()))


def dot(a, b, dims=(((1,), (0,)), ((), ()))):
    return lax.dot_general(a, b, dims, preferred_element_type=F32)


class Sems:
    def __init__(self, ref, size):
        self.ref, self.size, self.names = ref, size, {}

    def __getitem__(self, name):
        index = self.names.setdefault(name, len(self.names))
        assert index < self.size, index
        return self.ref.at[index]


def kernel(sizes, *refs):
    n, m, rows, srows, width = sizes
    chips, half_n, half_x = m // 2, n // 2, m // 4
    tgt, src = rows * m, srows * m
    (t_h, s_h, gain_h, wq_h, kw_h, vw_h, wo_h, saved_h, shift_h, og_h) = refs[:10]
    (tg_h, sg_h, wg_h) = refs[10:13]
    (
        t_v, s_v, gain_v, wq2, kw_v, vw_v, wo2, saved2, shift2,
        kinds, rows_all, rows_mat, nrm_mat, kvs, kv_all, k_t, blk, stg, stat_s, stat,
        acc, dqp, gp, d_snd, d_raw, d_sum, g_snd, g_raw, g_sum,
        pk_s, pk_r, ek_s, ek_r, dq_s, dq_r, f_s, f_r, tg_v, sg_v, wg_v,
        load_ref, send_ref, recv_ref, c_send, c_recv, st_send,
    ) = refs[13:]
    tp, sp = lax.axis_index("tp"), lax.axis_index("sp")
    x, c = tp // 2, tp % 2
    mate = x * 2 + 1 - c

    def chip(o):
        return (x + o + chips) % chips

    def ring(o):
        return (sp + o + n) % n

    loads, sends, recvs = Sems(load_ref, 16), Sems(send_ref, 400), Sems(recv_ref, 400)
    started = []

    def load(source, target, name):
        copy = pltpu.make_async_copy(source, target, loads[name])
        copy.start()
        return copy

    def send(source, target, name, device, key=None):
        copy = pltpu.make_async_remote_copy(
            src_ref=source, dst_ref=target, send_sem=sends[key or name + (len(started),)],
            recv_sem=recvs[name], device_id=device, device_id_type=pl.DeviceIdType.MESH,
        )
        copy.start()
        started.append(copy)

    def arrive(target, sem):
        pltpu.make_async_remote_copy(
            src_ref=target, dst_ref=target, send_sem=send_ref.at[0], recv_sem=sem,
            device_id={"tp": mate}, device_id_type=pl.DeviceIdType.MESH,
        ).wait_recv()

    get_t = load(t_h, t_v, "t")
    get_gain = load(gain_h, gain_v, "gain")
    get_og = load(og_h, kinds.at[1], "og")
    get_s = load(s_h, s_v, "s")
    get_kw = load(kw_h, kw_v, "kw")
    get_vw = load(vw_h, vw_v, "vw")
    get_wq = load(wq_h, wq2.at[:, 0:HEAD_DIM], "wq")
    get_wo = load(wo_h, wo2.at[0:HEAD_DIM], "wo")
    get_saved = load(saved_h, saved2.at[0], "saved")
    get_shift = load(shift_h, shift2.at[0], "shift")

    peers = [{"tp": chip(o) * 2 + c} for o in range(1, chips)]
    peers += [{"tp": chip(o) * 2 + 1 - c} for o in (-1, 0, 1)]
    peers += [{"sp": ring(o)} for o in (-2, -1, 1, 2)]
    peers += [{"sp": ring(o), "tp": mate} for o in (-1, 1)]
    barrier = pltpu.get_barrier_semaphore()
    for peer in peers:
        pl.semaphore_signal(barrier, inc=1, device_id=peer, device_id_type=pl.DeviceIdType.MESH)

    get_t.wait()
    get_gain.wait()
    wide = t_v[...].astype(F32)
    root = jnp.sqrt(jnp.mean(wide * wide, axis=1, keepdims=True) + 1e-06)
    kinds[0] = (wide / root * gain_v[...]).astype(BF16)
    get_og.wait()
    rows_all[tp] = kinds[c]
    pl.semaphore_wait(barrier, len(peers))

    part = width // A_SUBS
    cuts = [pl.ds(i * part, part) for i in range(A_SUBS)]
    for i, cut in enumerate(cuts):
        for way in (1, -1):
            if half_x == 0 or (half_x == 1 and (i < A_SUBS // 2) != (way == 1)):
                continue
            for k in (0, 1):
                copy = pltpu.make_async_remote_copy(
                    src_ref=kinds.at[k, :, cut], dst_ref=rows_all.at[tp, :, cut],
                    send_sem=sends["a1", i, way, k],
                    recv_sem=recv_ref.at[((way + 1) // 2 * A_SUBS + i) * 2 + c],
                    device_id={"tp": chip(way) * 2 + k}, device_id_type=pl.DeviceIdType.MESH,
                )
                copy.start()
                started.append(copy)
    for index in range(A_SUBS * 4):
        recvs["first", index]
    send(kinds.at[1 - c], rows_all.at[tp], ("mate_rows",), {"tp": mate})
    send(wq_h, wq2.at[:, HEAD_DIM : 2 * HEAD_DIM], ("wq",), {"tp": mate})
    send(wo_h, wo2.at[HEAD_DIM : 2 * HEAD_DIM], ("wo",), {"tp": mate})
    send(saved_h, saved2.at[1], ("saved",), {"tp": mate})
    send(shift_h, shift2.at[1], ("shift",), {"tp": mate})

    get_s.wait()
    get_kw.wait()
    get_vw.wait()
    keys = dot(s_v[...], kw_v[...]).astype(BF16)
    values = dot(s_v[...], vw_v[...]).astype(BF16)
    for g in range(KV_HEADS):
        piece = slice(g * HEAD_DIM, (g + 1) * HEAD_DIM)
        kvs[g, :, 0:HEAD_DIM] = keys[:, piece]
        kvs[g, :, HEAD_DIM:] = values[:, piece]

    def send_kv(o):
        to = chip(o)
        send(kvs.at[to // half_x], kv_all.at[tp], ("kv", o), {"tp": to * 2 + c})

    def a_arrive(hop, way, i):
        if hop == 1:
            for k in (0, 1):
                slot = chip(-way) * 2 + k
                arrive(
                    rows_all.at[slot, :, cuts[i]],
                    recv_ref.at[((way + 1) // 2 * A_SUBS + i) * 2 + k],
                )
        else:
            slot = chip(-way * hop) * 2
            arrive(rows_all.at[pl.ds(slot, 2), :, cuts[i]], recvs["a", hop, way, i])

    def a_on(hop, way, i):
        return hop < half_x_ring or (hop == half_x_ring and (i < A_SUBS // 2) == (way == 1))

    half_x_ring = chips // 2
    near = [o for k in range(1, half_x_ring + 1) for o in (k, -k)][: chips - 1]
    offsets = near[::-1]
    for hop in range(1, half_x_ring + 1):
        for i in range(A_SUBS):
            for way in (1, -1):
                if not a_on(hop, way, i):
                    continue
                a_arrive(hop, way, i)
                if a_on(hop + 1, way, i):
                    slot = chip(-way * hop) * 2
                    piece = rows_all.at[pl.ds(slot, 2), :, cuts[i]]
                    send(piece, piece, ("a", hop + 1, way, i), {"tp": chip(way) * 2 + c})
        if hop >= half_x_ring - 1:
            while offsets and (hop >= half_x_ring - 1):
                send_kv(offsets.pop(0))
        if hop == 1:
            kv_all[tp] = kvs[x // half_x]
            blk[:, 0:tgt, HEAD_DIM:] = jnp.zeros((n, tgt, HEAD_DIM), BF16)
            blk[:, tgt:, 0:HEAD_DIM] = jnp.zeros((n, tgt, HEAD_DIM), BF16)
            acc[...] = jnp.zeros(acc.shape, F32)
    arrive(rows_all.at[tp], recvs["mate_rows",])
    rows_mat[...] = rows_all[...].astype(F32).reshape(tgt, width).astype(BF16)
    get_wq.wait()
    get_wo.wait()
    get_saved.wait()
    get_shift.wait()
    for name, target in (
        ("wq", wq2.at[:, HEAD_DIM : 2 * HEAD_DIM]), ("wo", wo2.at[HEAD_DIM : 2 * HEAD_DIM]),
        ("saved", saved2.at[1]), ("shift", shift2.at[1]),
    ):
        arrive(target, recvs[name,])

    offset = math.log(n * src)

    @pl.when(c == 0)
    def _():
        both = dot(rows_mat[...], wq2[...]).astype(BF16)
        stg[0] = both[:, 0:HEAD_DIM]
        stg[1] = both[:, HEAD_DIM:]

    @pl.when(c == 1)
    def _():
        both = dot(rows_mat[...], wo2[...], NT).astype(BF16)
        stg[0] = both[:, 0:HEAD_DIM]
        stg[1] = both[:, HEAD_DIM:]
        for k in (0, 1):
            product = stg[k].astype(F32) * saved2[k].astype(F32)
            stat_s[k, 0:1, :] = (shift2[k] + offset) * LOG2E
            stat_s[k, 1:2, :] = jnp.sum(product.T, axis=0, keepdims=True)
        stat[sp] = stat_s[0]

    piece_rows = tgt // C_SUBS

    def c_piece(b, kind, i):
        return blk.at[
            b, pl.ds(kind * tgt + i * piece_rows, piece_rows), pl.ds(kind * HEAD_DIM, HEAD_DIM)
        ]

    c_copies, st_copies = [], []
    mine = pl.multiple_of(c * tgt, tgt)
    lane = pl.multiple_of(c * HEAD_DIM, HEAD_DIM)
    for i in range(C_SUBS):
        for way in (1, -1):
            for k in (0, 1):
                copy = pltpu.make_async_remote_copy(
                    src_ref=stg.at[k, pl.ds(i * piece_rows, piece_rows)],
                    dst_ref=blk.at[
                        sp,
                        pl.ds(pl.multiple_of(mine + i * piece_rows, piece_rows), piece_rows),
                        pl.ds(lane, HEAD_DIM),
                    ],
                    send_sem=c_send.at[(way + 1) // 2, i, k],
                    recv_sem=c_recv.at[(way + 1) // 2, 1, c, i],
                    device_id={"sp": ring(way), "tp": tp if k == 0 else mate},
                    device_id_type=pl.DeviceIdType.MESH,
                )
                copy.start()
                c_copies.append(copy)
    for way in (1, -1):
        for k in (0, 1):
            st_copies.append(
                pltpu.make_async_remote_copy(
                    src_ref=stat_s.at[k], dst_ref=stat.at[sp],
                    send_sem=st_send.at[(way + 1) // 2, k],
                    recv_sem=recvs["stat", way, 1],
                    device_id={"sp": ring(way), "tp": tp if k == 0 else mate},
                    device_id_type=pl.DeviceIdType.MESH,
                )
            )
    mate_stat = pltpu.make_async_remote_copy(
        src_ref=stat_s.at[1], dst_ref=stat.at[sp], send_sem=st_send.at[2, 0],
        recv_sem=recvs["mate_stat",], device_id={"tp": mate}, device_id_type=pl.DeviceIdType.MESH,
    )
    mate_rows = pltpu.make_async_remote_copy(
        src_ref=rows_mat, dst_ref=nrm_mat, send_sem=st_send.at[2, 1],
        recv_sem=recvs["nrm",], device_id={"tp": mate}, device_id_type=pl.DeviceIdType.MESH,
    )
    send(
        stg.at[1], blk.at[sp, pl.ds(mine, tgt), pl.ds(lane, HEAD_DIM)], ("mate_block",),
        {"tp": mate},
    )
    blk[sp, pl.ds(mine, tgt), pl.ds(lane, HEAD_DIM)] = stg[0]

    @pl.when(c == 1)
    def _():
        for copy in st_copies:
            copy.start()
        mate_stat.start()

    @pl.when(c == 0)
    def _():
        mate_rows.start()
        nrm_mat[...] = rows_mat[...]

    def c_on(hop, way, kind):
        return hop < half_n or (hop == half_n and (kind == 1) == (way == -1))

    def c_hop(hop):
        for i in range(C_SUBS):
            for kind in (0, 1):
                for way in (1, -1):
                    if not c_on(hop, way, kind):
                        continue
                    piece = c_piece(ring(-way * hop), kind, i)
                    arrive(piece, c_recv.at[(way + 1) // 2, hop, kind, i])
                    if c_on(hop + 1, way, kind):
                        copy = pltpu.make_async_remote_copy(
                            src_ref=piece, dst_ref=piece,
                            send_sem=sends["c", hop, kind, way, i],
                            recv_sem=c_recv.at[(way + 1) // 2, hop + 1, kind, i],
                            device_id={"sp": ring(way)}, device_id_type=pl.DeviceIdType.MESH,
                        )
                        copy.start()
                        started.append(copy)
        for way in (1, -1):
            if c_on(hop, way, 0):
                piece = stat.at[ring(-way * hop)]
                arrive(piece, recvs["stat", way, hop])
                if c_on(hop + 1, way, 0):
                    send(piece, piece, ("stat", way, hop + 1), {"sp": ring(way)})

    def kv_ready():
        for o in [0] + near:
            slot = kv_all.at[chip(-o) * 2 + c]
            if o != 0:
                arrive(slot, recvs["kv", o])
            send(slot, slot, ("kv_mate", o), {"tp": mate})
        for o in [0] + near:
            arrive(kv_all.at[chip(-o) * 2 + 1 - c], recvs["kv_mate", o])
        k_t[...] = kv_all[:, :, 0:HEAD_DIM].reshape(src, HEAD_DIM).T

        @pl.when(c == 0)
        def _():
            arrive(c_own(1), recvs["mate_block",])
            arrive(stat.at[sp], recvs["mate_stat",])

        @pl.when(c == 1)
        def _():
            arrive(c_own(0), recvs["mate_block",])

    def c_own(kind):
        return blk.at[sp, kind * tgt : (kind + 1) * tgt, kind * HEAD_DIM : (kind + 1) * HEAD_DIM]

    factor = HEAD_DIM ** (-0.5)
    tile = min(TILE, src)
    step = tile // srows

    def attend(index, carry):
        away = (index + 1) // 2 * (1 - 2 * (index % 2))
        b = (sp + away + n) % n
        block = blk[b]
        stats = stat[b]
        total = jnp.zeros((HEAD_DIM, tgt), F32)
        for at in range(0, m, step):
            kv = kv_all[at : at + step].reshape(tile, 2 * HEAD_DIM)
            both = dot(kv, block, NT)
            prob = jnp.exp2(both[:, 0:tgt] * (factor * LOG2E) - stats[0:1])
            grad = (prob * (both[:, tgt:] - stats[1:2])).astype(BF16)
            pair = jnp.concatenate([grad, prob.astype(BF16)], axis=1)
            added = dot(pair, block).reshape(step // 2, 2, srows, 2 * HEAD_DIM)
            acc[at // 2 : (at + step) // 2] += added
            total += dot(k_t[:, at * srows : at * srows + tile], grad)
        dqp[b] = total
        return carry

    done = 0
    for hop in range(1, half_n + 1):
        c_hop(hop)
        if hop == min(FIRST, half_n):
            kv_ready()
        if hop >= min(FIRST, half_n):
            have = n if hop == half_n else 1 + 2 * hop
            upto = have if hop == half_n else min(have, done + 4)
            lax.fori_loop(done, upto, attend, 0)
            done = upto

    def ring_sum(name, own, snd, raw, total, between):
        chunk = HEAD_DIM // R_SUBS
        limits = (half_n, half_n - 1)
        order = []
        for d in range(half_n, 0, -1):
            for side in (0, 1):
                if d <= limits[side]:
                    order.append((side, d))

        def block(side, d):
            return ring(-d if side == 0 else d)

        def put(side, d, i):
            cut = pl.ds(i * chunk, chunk)
            back = -1 if side == 0 else 1
            into = raw if d % 2 else total
            send(
                snd.at[side, d, cut], into.at[side, d, cut], (name, side, d, i),
                {"sp": ring(back if d % 2 else 2 * back)},
            )

        def term(side, d, i, value):
            cut = pl.ds(i * chunk, chunk)
            if d + 1 <= limits[side]:
                arrive(raw.at[side, d + 1, cut], recvs[name, side, d + 1, i])
                value += raw[side, d + 1, cut].astype(F32)
            if d + 2 <= limits[side]:
                arrive(total.at[side, d + 2, cut], recvs[name, side, d + 2, i])
                value += total[side, d + 2, cut].astype(F32)
            return value

        for side, d in order:
            if d % 2 or d == half_n:
                snd[side, d] = own(block(side, d), slice(None)).astype(BF16)
                for i in range(R_SUBS):
                    put(side, d, i)
        between(0)
        for stage, d in enumerate(range(half_n - 2, 0, -2)):
            if stage:
                between(stage)
            for i in range(R_SUBS):
                for side in (0, 1):
                    cut = pl.ds(i * chunk, chunk)
                    snd[side, d, cut] = term(side, d, i, own(block(side, d), cut)).astype(BF16)
                    put(side, d, i)
        for stage in range(max(1, half_n // 2 - 1), 4):
            between(stage)
        parts = []
        for i in range(R_SUBS):
            value = own(sp, pl.ds(i * chunk, chunk))
            for side in (0, 1):
                value = term(side, 0, i, value)
            parts.append(value)
        return jnp.concatenate(parts, axis=0)

    def own_dq(b, cut):
        return dqp[b, cut]

    def kv_pair(stage):
        if stage == 0:
            pk_s[...] = acc[:, 1 - c].astype(BF16)
            send(pk_s, pk_r, ("pk",), {"tp": mate})
        if stage == 1:
            arrive(pk_r, recvs["pk",])
            ek_s[...] = (acc[:, c] + pk_r[...].astype(F32)).astype(BF16)
            for o in near[::-1]:
                send(ek_s.at[chip(o)], ek_r.at[x], ("ek", o), {"tp": chip(o) * 2 + c})
            ek_r[x] = ek_s[x]

    dq_t = (ring_sum("d", own_dq, d_snd, d_raw, d_sum, kv_pair) * factor).astype(BF16)

    dq_rows = dq_t.astype(F32).T.reshape(chips, 2, rows, HEAD_DIM)
    dq_s[0] = dq_rows[:, 0].astype(BF16)
    dq_s[1] = dq_rows[:, 1].astype(BF16)
    send(dq_s.at[1 - c], dq_r, ("dq",), {"tp": mate})

    @pl.when(c == 1)
    def _():
        arrive(nrm_mat, recvs["nrm",])

    shares = dot(dq_t, nrm_mat[...])
    cols = width // n
    for b in range(n):
        gp[b] = shares[:, b * cols : (b + 1) * cols]

    def row_share():
        arrive(dq_r, recvs["dq",])
        left = dq_s[c].astype(F32).reshape(chips * rows, HEAD_DIM).astype(BF16)
        right = dq_r[...].astype(F32).reshape(chips * rows, HEAD_DIM).astype(BF16)
        share = dot(jnp.concatenate([left, right], axis=1), wq2[...], NT)
        f_s[...] = share.reshape(chips, rows, width).astype(BF16)
        for o in near[::-1]:
            send(f_s.at[chip(o)], f_r.at[x], ("f", o), {"tp": chip(o) * 2 + c})
        f_r[x] = f_s[x]

    put_sg = pltpu.make_async_copy(sg_v, sg_h, loads["sg"])
    put_tg = pltpu.make_async_copy(tg_v, tg_h, loads["tg"])
    put_wg = pltpu.make_async_copy(wg_v, wg_h, loads["wg"])

    def source_out():
        for o in near:
            arrive(ek_r.at[chip(-o)], recvs["ek", o])
        sums = [
            jnp.sum(ek_r[g * half_x : (g + 1) * half_x].astype(F32), axis=0)
            for g in range(KV_HEADS)
        ]
        dk = jnp.concatenate([s[:, 0:HEAD_DIM] * factor for s in sums], axis=1).astype(BF16)
        dv = jnp.concatenate([s[:, HEAD_DIM:] for s in sums], axis=1).astype(BF16)
        sg_v[...] = dot(dk, kw_v[...], NT) + dot(dv, vw_v[...], NT)
        put_sg.start()

    def target_out():
        for o in near:
            arrive(f_r.at[chip(-o)], recvs["f", o])
        grad = jnp.sum(f_r[...].astype(F32), axis=0)
        wide = t_v[...].astype(F32)
        root = jnp.sqrt(jnp.mean(wide * wide, axis=1, keepdims=True) + 1e-06)
        scaled = grad * gain_v[...]
        mean = jnp.mean(scaled * wide, axis=1, keepdims=True)
        tg_v[...] = scaled / root - wide * mean / (root * root * root)
        put_tg.start()

    def rest(stage):
        if stage == 0:
            row_share()
        if stage == 1:
            source_out()
        if stage == 3:
            target_out()

    def own_g(b, cut):
        return gp[b, cut]

    wg_v[...] = ring_sum("g", own_g, g_snd, g_raw, g_sum, rest).T
    put_wg.start()
    for copy in started:
        copy.wait_send()
    for copy in c_copies:
        copy.wait_send()

    @pl.when(c == 1)
    def _():
        for copy in st_copies:
            copy.wait_send()
        mate_stat.wait_send()

    @pl.when(c == 0)
    def _():
        mate_rows.wait_send()

    put_sg.wait()
    put_tg.wait()
    put_wg.wait()


def shards(
    target, source, norm_gain, query_weight, key_weight, value_weight, output_weight, saved_out,
    log_shift, out_grad,
):
    n, m = lax.axis_size("sp"), lax.axis_size("tp")
    rows, width = target.shape
    srows = source.shape[0]
    chips, tgt, src = m // 2, rows * m, srows * m
    cols = width // n
    half = n // 2 + 1
    hd = HEAD_DIM
    vmem = pltpu.VMEM
    scratch = [
        vmem((rows, width), BF16),
        vmem((srows, width), BF16),
        vmem((1, width), F32),
        vmem((width, 2 * hd), BF16),
        vmem((width, KV_HEADS * hd), BF16),
        vmem((width, KV_HEADS * hd), BF16),
        vmem((2 * hd, width), BF16),
        vmem((2, tgt, hd), BF16),
        vmem((2, 1, tgt), F32),
        vmem((2, rows, width), BF16),
        vmem((m, rows, width), BF16),
        vmem((tgt, width), BF16),
        vmem((tgt, width), BF16),
        vmem((KV_HEADS, srows, 2 * hd), BF16),
        vmem((m, srows, 2 * hd), BF16),
        vmem((hd, src), BF16),
        vmem((n, 2 * tgt, 2 * hd), BF16),
        vmem((2, tgt, hd), BF16),
        vmem((2, 2, tgt), F32),
        vmem((n, 2, tgt), F32),
        vmem((chips, 2, srows, 2 * hd), F32),
        vmem((n, hd, tgt), F32),
        vmem((n, hd, cols), F32),
        *[vmem((2, half, hd, tgt), BF16)] * 3,
        *[vmem((2, half, hd, cols), BF16)] * 3,
        *[vmem((chips, srows, 2 * hd), BF16)] * 4,
        vmem((2, chips, rows, hd), BF16),
        vmem((chips, rows, hd), BF16),
        *[vmem((chips, rows, width), BF16)] * 2,
        vmem((rows, width), F32),
        vmem((srows, width), F32),
        vmem((cols, hd), F32),
        pltpu.SemaphoreType.DMA((16,)),
        pltpu.SemaphoreType.DMA((400,)),
        pltpu.SemaphoreType.DMA((400,)),
        pltpu.SemaphoreType.DMA((2, C_SUBS, 2)),
        pltpu.SemaphoreType.DMA((2, half, 2, C_SUBS)),
        pltpu.SemaphoreType.DMA((3, 2)),
    ]
    anywhere = pl.BlockSpec(memory_space=pl.ANY)
    return pl.pallas_call(
        functools.partial(kernel, (n, m, rows, srows, width)),
        out_shape=(
            jax.ShapeDtypeStruct((rows, width), F32),
            jax.ShapeDtypeStruct((srows, width), F32),
            jax.ShapeDtypeStruct((cols, hd), F32),
        ),
        in_specs=[anywhere] * 10,
        out_specs=(anywhere,) * 3,
        scratch_shapes=scratch,
        compiler_params=pltpu.CompilerParams(
            collective_id=0, has_side_effects=True, vmem_limit_bytes=48 * 1024 * 1024
        ),
    )(
        target, source, norm_gain.reshape(1, width), query_weight, key_weight, value_weight,
        output_weight, saved_out, log_shift, out_grad,
    )


def solution(mesh):
    return jax.shard_map(
        shards,
        mesh=mesh,
        in_specs=(
            P(("grp", "sp", "tp"), None),
            P(("grp", "sp", "tp"), None),
            P(),
            P(None, "tp"),
            P(),
            P(),
            P("tp", None),
            P(("grp", "sp"), "tp"),
            P("tp", ("grp", "sp")),
            P(("grp", "sp", "tp"), None),
        ),
        out_specs=(
            P(("grp", "sp", "tp"), None),
            P(("grp", "sp", "tp"), None),
            P(("grp", "sp"), "tp"),
        ),
        check_vma=False,
    )
```

time: 310 us -> 144 us (0.46); the launches traced: 305 us -> 143 us
  blocking collectives: 160 us -> 0 us
  Pallas kernels: 0 us -> 131 us
  waiting for transfers between devices: 63.4 us -> 0 us
  matrix products: 26.5 us -> 0 us
  starting transfers between devices: 24 us -> 0 us
  between operations: 14.3 us -> 0.66 us
  other arithmetic: 8.83 us -> 0 us
  local copies, waits for them, and re-layouts: 7.35 us -> 11.2 us
    all_gather x4 -> x0, blocking collectives: 160 us -> none  [the longest x1 68 us: shards(): lax.all_gather(shift_cols.astype(jnp.bfloat16), 'sp', axis=0, tiled=True)]
    pallas_call x0 -> x1, Pallas kernels: none -> 131 us  [shards(): pl.pallas_call(functools.partial(kernel, (n, m, rows, srows, width)), out...]
    all_to_all x4 -> x0, waiting for transfers between devices: 56.9 us -> none  [the longest x3 42.3 us: summed_on_arrival(): lax.all_to_all(blocks, axis, split_axis=0, concat_axis=0, tiled=True)]
    dot_general x12 -> x0, matrix products: 26.5 us -> none  [the longest x1 5.33 us: shards(): jnp.einsum('hnm,nhd->md', prob_low, back_three, preferred_element_type=jn...]
    all_to_all x4 -> x0, starting transfers between devices: 23.9 us -> none  [the longest x3 19.2 us: summed_on_arrival(): lax.all_to_all(blocks, axis, split_axis=0, concat_axis=0, tiled=True)]
    unnamed x21 -> x23, local copies, waits for them, and re-layouts: 4.63 us -> 11.2 us
    all_gather x2 -> x0, waiting for transfers between devices: 5.75 us -> none  [the longest x1 5.75 us: shards(): portion = lax.all_gather(joined, 'tp', axis=0, tiled=True)]
    reduce_sum x6 -> x0, other arithmetic: 4.09 us -> none  [the longest x3 2.95 us: summed_on_arrival(): return arrived.astype(jnp.float32).sum(axis=0)]
  transfers between devices with their start and end apart: 6 -> 0, of which waited for: 5 -> 0; matrix products, arithmetic and copies ran while one was open for 9% -> 0% of each run, Pallas kernels for 0% -> 0%
where the time goes in v1:
time: 144 us; the launch traced here: 143 us
  Pallas kernels  131 us (91%)
  local copies, waits for them, and re-layouts  11.2 us (8%)
    pallas_call x1, Pallas kernels, shards(): pl.pallas_call(functools.partial(kernel, (n, m, rows, srows, width)), out...  131 us
    unnamed x23, local copies, waits for them, and re-layouts  11.2 us

profile of v1, /device:TPU:80, one launch (start us, length us, event | category | flops | bytes accessed | tf_op | source)
XLA Modules:
  0.0 143.1 jit_solution(9219835221046770628)
XLA Ops:
  0.6 0.0 copy-start.9
  0.6 0.6 copy-done.9
  1.3 0.0 copy-start
  1.3 1.2 copy-done
  2.5 0.0 copy-start.1
  2.5 1.2 copy-done.1
  3.7 0.0 copy-start.2
  3.7 1.0 copy-done.2
  4.8 0.0 copy-start.3
  4.8 1.0 copy-done.3
  5.8 0.0 copy-start.4
  5.8 0.9 copy-done.4
  6.8 0.0 copy-start.5
  6.8 0.8 copy-done.5
  7.5 0.0 copy-start.6
  7.5 0.8 copy-done.6
  8.3 0.0 copy-start.7
  8.3 0.8 copy-done.7
  9.1 0.0 copy-start.8
  9.1 0.7 copy-done.8
  9.7 131.3 %shard_map.121 = (f32[8,2048]{1,0:T(8,128)S(1)}, f32[64,2048]{1,0:T(8,128)S(1)}, f32[128,128]{1,0:T(8,128)S(1)}) custom-call(bf16[8,2048]{1,0:T(8,128)(2,1)S(1)} %copy-done.5, bf16[64,2048]{1,0:T(8,128)(2,1)S(1)} %copy-done.4, f32[1,2048]{1,0:T(1,128)S(1)} %bitcast.1, bf16[2048,128]{1,0:T(8,128)(2,1)S(1)} %copy-done.2, bf16[2048,256]{1,0:T(8,128)(2,1)S(1)} %copy-done, ...), custom_call_target="tpu_custom_call" | custom-call | tf_op jit(solution)/shard_map/pallas_call | solution.py:567
  141.1 0.6 copy.16
  141.7 0.8 copy.17
  142.5 0.6 copy.18
Async XLA Ops:
  0.6 0.7 copy-start.9
  1.3 1.2 copy-start
  2.5 1.2 copy-start.1
  3.7 1.0 copy-start.2
  4.8 1.0 copy-start.3
  5.8 0.9 copy-start.4
  6.8 0.8 copy-start.5
  7.5 0.8 copy-start.6
  8.3 0.8 copy-start.7
  9.1 0.7 copy-start.8

commit v2 on v1

v2 whole, which is shorter than its diff:
```python
import functools
import math

import jax
import jax.numpy as jnp
from jax import lax
from jax.experimental import pallas as pl
from jax.experimental.pallas import tpu as pltpu
from jax.sharding import PartitionSpec as P

HEAD_DIM = 128
KV_HEADS = 2
A_SUBS = 2
C_SUBS = 2
R_SUBS = 2
TILE = 512
LOG2E = math.log2(math.e)
F32, BF16 = jnp.float32, jnp.bfloat16
NT = (((1,), (1,)), ((), ()))


def dot(a, b, dims=(((1,), (0,)), ((), ()))):
    return lax.dot_general(a, b, dims, preferred_element_type=F32)


class Sems:
    def __init__(self, ref):
        self.ref, self.names = ref, {}

    def __getitem__(self, name):
        index = self.names.setdefault(name, len(self.names))
        assert index < self.ref.shape[0], index
        return self.ref.at[index]


def size_of(ref):
    return math.prod(ref.shape) * jnp.dtype(ref.dtype).itemsize


def kernel(sizes, *refs):
    n, m, rows, srows, width = sizes
    chips, half_n, half_x = m // 2, n // 2, m // 4
    tgt, src = rows * m, srows * m
    (t_h, s_h, gain_h, wq_h, kw_h, vw_h, wo_h, saved_h, shift_h, og_h) = refs[:10]
    (tg_h, sg_h, wg_h) = refs[10:13]
    (
        t_v, s_v, gain_v, wq2, kw_v, vw_v, wo2, saved2, shift2,
        kinds, rows_all, rows_mat, nrm_mat, kvs, kv_all, k_t, blk, stg, stat_s, stat,
        acc, dqp, gp, d_snd, d_raw, d_sum, g_snd, g_raw, g_sum,
        pk_s, pk_r, ek_s, ek_r, dq_s, dq_r, f_s, f_r, tg_v, sg_v, wg_v,
        ruler, load_ref, send_ref, recv_ref,
    ) = refs[13:]
    tp, sp = lax.axis_index("tp"), lax.axis_index("sp")
    x, c = tp // 2, tp % 2
    mate = x * 2 + 1 - c

    def chip(o):
        return (x + o + chips) % chips

    def ring(o):
        return (sp + o + n) % n

    loads, sends, recvs = Sems(load_ref), Sems(send_ref), Sems(recv_ref)
    sent = {}

    def remote(source, target, group, name, device):
        return pltpu.make_async_remote_copy(
            src_ref=source, dst_ref=target, send_sem=sends[group], recv_sem=recvs[name],
            device_id=device, device_id_type=pl.DeviceIdType.MESH,
        )

    def load(source, target, name):
        copy = pltpu.make_async_copy(source, target, loads[name])
        copy.start()
        return copy

    def send(source, target, group, name, device):
        remote(source, target, group, name, device).start()
        sent[group] = sent.get(group, 0) + size_of(source)

    def arrive(target, *name):
        remote(target, target, "a", name, {"tp": mate}).wait_recv()

    def length(size):
        return ruler.at[pl.ds(0, size // (2 * 128 * 4))]

    get_t = load(t_h, t_v, "t")
    get_gain = load(gain_h, gain_v, "gain")
    get_og = load(og_h, kinds.at[1], "og")
    get_s = load(s_h, s_v, "s")
    get_kw = load(kw_h, kw_v, "kw")
    get_vw = load(vw_h, vw_v, "vw")
    get_wq = load(wq_h, wq2.at[:, 0:HEAD_DIM], "wq")
    get_wo = load(wo_h, wo2.at[0:HEAD_DIM], "wo")
    get_saved = load(saved_h, saved2.at[0], "saved")
    get_shift = load(shift_h, shift2.at[0], "shift")

    peers = [{"tp": chip(o) * 2 + c} for o in range(1, chips)]
    peers += [{"tp": chip(o) * 2 + 1 - c} for o in (-2, -1, 0, 1, 2)]
    peers += [{"sp": ring(o), "tp": j} for o in (-2, -1, 1, 2) for j in (tp, mate)]
    barrier = pltpu.get_barrier_semaphore()
    for peer in peers:
        pl.semaphore_signal(barrier, inc=1, device_id=peer, device_id_type=pl.DeviceIdType.MESH)

    get_t.wait()
    get_gain.wait()
    wide = t_v[...].astype(F32)
    root = jnp.sqrt(jnp.mean(wide * wide, axis=1, keepdims=True) + 1e-06)
    kinds[0] = (wide / root * gain_v[...]).astype(BF16)
    get_og.wait()
    rows_all[tp] = kinds[c]
    pl.semaphore_wait(barrier, len(peers))

    half_x_ring = chips // 2
    part = width // A_SUBS
    cuts = [pl.ds(i * part, part) for i in range(A_SUBS)]

    def a_far(way, i):
        return half_x_ring - ((i < A_SUBS // 2) != (way == 1))

    for i, cut in enumerate(cuts):
        for d in (2, 1):
            for way in (1, -1):
                if d <= a_far(way, i):
                    for k in (0, 1):
                        send(
                            kinds.at[k, :, cut], rows_all.at[tp, :, cut], "a", ("a", way, d, i),
                            {"tp": chip(way * d) * 2 + k},
                        )
    send(kinds.at[1 - c], rows_all.at[tp], "a", ("mate_rows",), {"tp": mate})
    send(wq_h, wq2.at[:, HEAD_DIM : 2 * HEAD_DIM], "wq", ("wq",), {"tp": mate})
    send(wo_h, wo2.at[HEAD_DIM : 2 * HEAD_DIM], "wo", ("wo",), {"tp": mate})
    send(saved_h, saved2.at[1], "saved", ("saved",), {"tp": mate})
    send(shift_h, shift2.at[1], "shift", ("shift",), {"tp": mate})

    get_s.wait()
    get_kw.wait()
    get_vw.wait()
    keys = dot(s_v[...], kw_v[...]).astype(BF16)
    values = dot(s_v[...], vw_v[...]).astype(BF16)
    for g in range(KV_HEADS):
        piece = slice(g * HEAD_DIM, (g + 1) * HEAD_DIM)
        kvs[g, :, 0:HEAD_DIM] = keys[:, piece]
        kvs[g, :, HEAD_DIM:] = values[:, piece]

    near = [o for k in range(1, half_x_ring + 1) for o in (k, -k)][: chips - 1]
    for d in range(2, half_x_ring + 2, 2):
        for i, cut in enumerate(cuts):
            for way in (1, -1):
                if d > a_far(way, i):
                    continue
                piece = rows_all.at[pl.ds(chip(-way * d) * 2, 2), :, cut]
                arrive(piece, "a", way, d, i)
                for more in (2, 1):
                    if d + more <= a_far(way, i):
                        send(
                            piece, piece, "a", ("a", way, d + more, i),
                            {"tp": chip(way * more) * 2 + c},
                        )
        if d == 2:
            for o in near[::-1]:
                to = chip(o)
                send(kvs.at[to // half_x], kv_all.at[tp], "kv", ("kv", o), {"tp": to * 2 + c})
            kv_all[tp] = kvs[x // half_x]
            blk[:, 0:tgt, HEAD_DIM:] = jnp.zeros((n, tgt, HEAD_DIM), BF16)
            blk[:, tgt:, 0:HEAD_DIM] = jnp.zeros((n, tgt, HEAD_DIM), BF16)
            acc[...] = jnp.zeros(acc.shape, F32)
    for d in range(1, half_x_ring + 1, 2):
        for i, cut in enumerate(cuts):
            for way in (1, -1):
                if d <= a_far(way, i):
                    arrive(rows_all.at[pl.ds(chip(-way * d) * 2, 2), :, cut], "a", way, d, i)
    arrive(rows_all.at[tp], "mate_rows")
    rows_mat[...] = rows_all[...].astype(F32).reshape(tgt, width).astype(BF16)
    get_wq.wait()
    get_wo.wait()
    get_saved.wait()
    get_shift.wait()
    for name, target in (
        ("wq", wq2.at[:, HEAD_DIM : 2 * HEAD_DIM]), ("wo", wo2.at[HEAD_DIM : 2 * HEAD_DIM]),
        ("saved", saved2.at[1]), ("shift", shift2.at[1]),
    ):
        arrive(target, name)

    offset = math.log(n * src)

    @pl.when(c == 0)
    def _():
        both = dot(rows_mat[...], wq2[...]).astype(BF16)
        stg[0] = both[:, 0:HEAD_DIM]
        stg[1] = both[:, HEAD_DIM:]

    @pl.when(c == 1)
    def _():
        both = dot(rows_mat[...], wo2[...], NT).astype(BF16)
        stg[0] = both[:, 0:HEAD_DIM]
        stg[1] = both[:, HEAD_DIM:]
        for k in (0, 1):
            product = stg[k].astype(F32) * saved2[k].astype(F32)
            stat_s[k, 0:1, :] = (shift2[k] + offset) * LOG2E
            stat_s[k, 1:2, :] = jnp.sum(product.T, axis=0, keepdims=True)
        stat[sp] = stat_s[0]

    piece_rows = tgt // C_SUBS

    def c_piece(b, kind, i):
        return blk.at[
            b, pl.ds(kind * tgt + i * piece_rows, piece_rows), pl.ds(kind * HEAD_DIM, HEAD_DIM)
        ]


    def c_far(way, kind):
        return half_n - ((kind == 0) != (way == 1))

    mine = pl.multiple_of(c * tgt, tgt)
    lane = pl.multiple_of(c * HEAD_DIM, HEAD_DIM)
    own_lane = pl.ds(lane, HEAD_DIM)
    for i in range(C_SUBS):
        own_rows = pl.ds(pl.multiple_of(mine + i * piece_rows, piece_rows), piece_rows)
        for d in (2, 1):
            for way in (1, -1):
                for k in (0, 1):
                    send(
                        stg.at[k, pl.ds(i * piece_rows, piece_rows)],
                        blk.at[sp, own_rows, own_lane], "c", ("c", way, d, i),
                        {"sp": ring(way * d), "tp": tp if k == 0 else mate},
                    )
    own_stats = [
        remote(
            stat_s.at[k], stat.at[sp], "own_stat", ("stat", way, d),
            {"sp": ring(way * d), "tp": tp if k == 0 else mate},
        )
        for d in (2, 1) for way in (1, -1) for k in (0, 1)
    ]
    mate_stat = remote(stat_s.at[1], stat.at[sp], "mate_stat", ("mate_stat",), {"tp": mate})
    mate_rows = remote(rows_mat, nrm_mat, "nrm", ("nrm",), {"tp": mate})
    send(stg.at[1], blk.at[sp, pl.ds(mine, tgt), own_lane], "c", ("mate_block",), {"tp": mate})
    blk[sp, pl.ds(mine, tgt), own_lane] = stg[0]

    @pl.when(c == 1)
    def _():
        for copy in own_stats:
            copy.start()
        mate_stat.start()

    @pl.when(c == 0)
    def _():
        mate_rows.start()
        nrm_mat[...] = rows_mat[...]

    def c_arrive(way, d, i):
        b = ring(-way * d)
        kinds_here = [kind for kind in (0, 1) if d <= c_far(way, kind)]
        rows_here = len(kinds_here) * piece_rows
        arrive(blk.at[b, pl.ds(0, rows_here), pl.ds(0, HEAD_DIM)], "c", way, d, i)
        return b, kinds_here

    def c_even(d):
        for i in range(C_SUBS):
            for way in (1, -1):
                b, kinds_here = c_arrive(way, d, i)
                for more in (2, 1):
                    for kind in kinds_here:
                        if d + more <= c_far(way, kind):
                            piece = c_piece(b, kind, i)
                            send(
                                piece, piece, "c", ("c", way, d + more, i),
                                {"sp": ring(way * more)},
                            )
        for way in (1, -1):
            if d <= c_far(way, 0):
                piece = stat.at[ring(-way * d)]
                arrive(piece, "stat", way, d)
                for more in (2, 1):
                    if d + more <= c_far(way, 0):
                        send(piece, piece, "stat", ("stat", way, d + more), {"sp": ring(way * more)})

    def c_odd(d):
        for way in (1, -1):
            for i in range(C_SUBS):
                c_arrive(way, d, i)
            arrive(stat.at[ring(-way * d)], "stat", way, d)

    def kv_pass():
        for o in [0] + near:
            slot = kv_all.at[chip(-o) * 2 + c]
            if o != 0:
                arrive(slot, "kv", o)
            send(slot, slot, "kv", ("kv_mate",), {"tp": mate})

    def kv_ready():
        arrive(kv_all.at[pl.ds(0, chips)], "kv_mate")
        k_t[...] = kv_all[:, :, 0:HEAD_DIM].reshape(src, HEAD_DIM).T

        @pl.when(c == 0)
        def _():
            arrive(c_own(1), "mate_block")
            arrive(stat.at[sp], "mate_stat")

        @pl.when(c == 1)
        def _():
            arrive(c_own(0), "mate_block")

    def c_own(kind):
        return blk.at[sp, kind * tgt : (kind + 1) * tgt, kind * HEAD_DIM : (kind + 1) * HEAD_DIM]

    factor = HEAD_DIM ** (-0.5)
    tile = min(TILE, src)
    step = tile // srows

    def attend(index, carry):
        away = (index + 1) // 2 * (1 - 2 * (index % 2))
        b = (sp + away + n) % n
        block = blk[b]
        stats = stat[b]
        total = jnp.zeros((HEAD_DIM, tgt), F32)
        for at in range(0, m, step):
            kv = kv_all[at : at + step].reshape(tile, 2 * HEAD_DIM)
            both = dot(kv, block, NT)
            prob = jnp.exp2(both[:, 0:tgt] * (factor * LOG2E) - stats[0:1])
            grad = (prob * (both[:, tgt:] - stats[1:2])).astype(BF16)
            pair = jnp.concatenate([grad, prob.astype(BF16)], axis=1)
            added = dot(pair, block).reshape(step // 2, 2, srows, 2 * HEAD_DIM)
            acc[at // 2 : (at + step) // 2] += added
            total += dot(k_t[:, at * srows : at * srows + tile], grad)
        dqp[b] = total
        return carry

    done = 0
    kv_pass()
    for d in range(2, half_n + 2, 2):
        c_even(d)
        if d == 2:
            kv_ready()
        c_odd(d - 1)
        upto = n if d == half_n else min(done + 4, 1 + 2 * d)
        lax.fori_loop(done, upto, attend, 0)
        done = upto

    def ring_sum(name, own, snd, raw, total, between):
        chunk = HEAD_DIM // R_SUBS
        limits = (half_n, half_n - 1)
        order = []
        for d in range(half_n, 0, -1):
            for side in (0, 1):
                if d <= limits[side]:
                    order.append((side, d))

        def block(side, d):
            return ring(-d if side == 0 else d)

        def put(side, d, i):
            cut = pl.ds(i * chunk, chunk)
            back = -1 if side == 0 else 1
            into = raw if d % 2 else total
            send(
                snd.at[side, d, cut], into.at[side, d, cut], name,
                (name, side, (d - 1) // 2, i), {"sp": ring(back if d % 2 else 2 * back)},
            )

        def term(side, d, i, value):
            cut = pl.ds(i * chunk, chunk)
            arrive(raw.at[side, pl.ds(0, 1 + (d + 2 <= limits[side])), cut], name, side, d // 2, i)
            value += raw[side, d + 1, cut].astype(F32)
            if d + 2 <= limits[side]:
                value += total[side, d + 2, cut].astype(F32)
            return value

        for side, d in order:
            if d % 2 or d == half_n:
                snd[side, d] = own(block(side, d), slice(None)).astype(BF16)
                for i in range(R_SUBS):
                    put(side, d, i)
        between(0)
        for stage, d in enumerate(range(half_n - 2, 0, -2)):
            if stage:
                between(stage)
            for i in range(R_SUBS):
                for side in (0, 1):
                    cut = pl.ds(i * chunk, chunk)
                    snd[side, d, cut] = term(side, d, i, own(block(side, d), cut)).astype(BF16)
                    put(side, d, i)
        for stage in range(max(1, half_n // 2 - 1), 4):
            between(stage)
        parts = []
        for i in range(R_SUBS):
            value = own(sp, pl.ds(i * chunk, chunk))
            for side in (0, 1):
                value = term(side, 0, i, value)
            parts.append(value)
        return jnp.concatenate(parts, axis=0)

    def own_dq(b, cut):
        return dqp[b, cut]

    def kv_pair(stage):
        if stage == 0:
            pk_s[...] = acc[:, 1 - c].astype(BF16)
            send(pk_s, pk_r, "pk", ("pk",), {"tp": mate})
        if stage == 1:
            arrive(pk_r, "pk")
            ek_s[...] = (acc[:, c] + pk_r[...].astype(F32)).astype(BF16)
            for o in near[::-1]:
                send(ek_s.at[chip(o)], ek_r.at[x], "ek", ("ek",), {"tp": chip(o) * 2 + c})
            ek_r[x] = ek_s[x]

    dq_t = (ring_sum("d", own_dq, d_snd, d_raw, d_sum, kv_pair) * factor).astype(BF16)

    dq_rows = dq_t.astype(F32).T.reshape(chips, 2, rows, HEAD_DIM)
    dq_s[0] = dq_rows[:, 0].astype(BF16)
    dq_s[1] = dq_rows[:, 1].astype(BF16)
    send(dq_s.at[1 - c], dq_r, "dq", ("dq",), {"tp": mate})

    @pl.when(c == 1)
    def _():
        arrive(nrm_mat, "nrm")

    shares = dot(dq_t, nrm_mat[...])
    cols = width // n
    for b in range(n):
        gp[b] = shares[:, b * cols : (b + 1) * cols]

    def row_share():
        arrive(dq_r, "dq")
        left = dq_s[c].astype(F32).reshape(chips * rows, HEAD_DIM).astype(BF16)
        right = dq_r[...].astype(F32).reshape(chips * rows, HEAD_DIM).astype(BF16)
        share = dot(jnp.concatenate([left, right], axis=1), wq2[...], NT)
        f_s[...] = share.reshape(chips, rows, width).astype(BF16)
        for o in near[::-1]:
            send(f_s.at[chip(o)], f_r.at[x], "f", ("f",), {"tp": chip(o) * 2 + c})
        f_r[x] = f_s[x]

    put_sg = pltpu.make_async_copy(sg_v, sg_h, loads["sg"])
    put_tg = pltpu.make_async_copy(tg_v, tg_h, loads["tg"])
    put_wg = pltpu.make_async_copy(wg_v, wg_h, loads["wg"])

    def source_out():
        arrive(ek_r.at[pl.ds(0, chips - 1)], "ek")
        sums = [
            jnp.sum(ek_r[g * half_x : (g + 1) * half_x].astype(F32), axis=0)
            for g in range(KV_HEADS)
        ]
        dk = jnp.concatenate([s[:, 0:HEAD_DIM] * factor for s in sums], axis=1).astype(BF16)
        dv = jnp.concatenate([s[:, HEAD_DIM:] for s in sums], axis=1).astype(BF16)
        sg_v[...] = dot(dk, kw_v[...], NT) + dot(dv, vw_v[...], NT)
        put_sg.start()

    def target_out():
        arrive(f_r.at[pl.ds(0, chips - 1)], "f")
        grad = jnp.sum(f_r[...].astype(F32), axis=0)
        wide = t_v[...].astype(F32)
        root = jnp.sqrt(jnp.mean(wide * wide, axis=1, keepdims=True) + 1e-06)
        scaled = grad * gain_v[...]
        mean = jnp.mean(scaled * wide, axis=1, keepdims=True)
        tg_v[...] = scaled / root - wide * mean / (root * root * root)
        put_tg.start()

    def rest(stage):
        if stage == 1:
            row_share()
        if stage == 2:
            source_out()
        if stage == 3:
            target_out()

    def own_g(b, cut):
        return gp[b, cut]

    wg_v[...] = ring_sum("g", own_g, g_snd, g_raw, g_sum, rest).T
    put_wg.start()
    sources = {"wq": wq_h, "wo": wo_h, "saved": saved_h, "shift": shift_h}
    for group, size in sent.items():
        whole = sources.get(group) if group in sources else length(size)
        remote(whole, whole, group, ("pk",), {"tp": mate}).wait_send()

    @pl.when(c == 1)
    def _():
        whole = length(len(own_stats) * size_of(stat_s.at[0]))
        remote(whole, whole, "own_stat", ("pk",), {"tp": mate}).wait_send()
        mate_stat.wait_send()

    @pl.when(c == 0)
    def _():
        mate_rows.wait_send()

    put_sg.wait()
    put_tg.wait()
    put_wg.wait()


def shards(
    target, source, norm_gain, query_weight, key_weight, value_weight, output_weight, saved_out,
    log_shift, out_grad,
):
    n, m = lax.axis_size("sp"), lax.axis_size("tp")
    rows, width = target.shape
    srows = source.shape[0]
    chips, tgt, src = m // 2, rows * m, srows * m
    cols = width // n
    half = n // 2 + 1
    hd = HEAD_DIM
    vmem = pltpu.VMEM
    scratch = [
        vmem((rows, width), BF16),
        vmem((srows, width), BF16),
        vmem((1, width), F32),
        vmem((width, 2 * hd), BF16),
        vmem((width, KV_HEADS * hd), BF16),
        vmem((width, KV_HEADS * hd), BF16),
        vmem((2 * hd, width), BF16),
        vmem((2, tgt, hd), BF16),
        vmem((2, 1, tgt), F32),
        vmem((2, rows, width), BF16),
        vmem((m, rows, width), BF16),
        vmem((tgt, width), BF16),
        vmem((tgt, width), BF16),
        vmem((KV_HEADS, srows, 2 * hd), BF16),
        vmem((m, srows, 2 * hd), BF16),
        vmem((hd, src), BF16),
        vmem((n, 2 * tgt, 2 * hd), BF16),
        vmem((2, tgt, hd), BF16),
        vmem((2, 2, tgt), F32),
        vmem((n, 2, tgt), F32),
        vmem((chips, 2, srows, 2 * hd), F32),
        vmem((n, hd, tgt), F32),
        vmem((n, hd, cols), F32),
        *[vmem((2, half, hd, tgt), BF16)] * 3,
        *[vmem((2, half, hd, cols), BF16)] * 3,
        *[vmem((chips, srows, 2 * hd), BF16)] * 4,
        vmem((2, chips, rows, hd), BF16),
        vmem((chips, rows, hd), BF16),
        *[vmem((chips, rows, width), BF16)] * 2,
        vmem((rows, width), F32),
        vmem((srows, width), F32),
        vmem((cols, hd), F32),
        vmem((1024, 2, 128), F32),
        pltpu.SemaphoreType.DMA((13,)),
        pltpu.SemaphoreType.DMA((17,)),
        pltpu.SemaphoreType.DMA((113,)),
    ]
    anywhere = pl.BlockSpec(memory_space=pl.ANY)
    return pl.pallas_call(
        functools.partial(kernel, (n, m, rows, srows, width)),
        out_shape=(
            jax.ShapeDtypeStruct((rows, width), F32),
            jax.ShapeDtypeStruct((srows, width), F32),
            jax.ShapeDtypeStruct((cols, hd), F32),
        ),
        in_specs=[anywhere] * 10,
        out_specs=(anywhere,) * 3,
        scratch_shapes=scratch,
        compiler_params=pltpu.CompilerParams(
            collective_id=0, has_side_effects=True, vmem_limit_bytes=64_000_000
        ),
    )(
        target, source, norm_gain.reshape(1, width), query_weight, key_weight, value_weight,
        output_weight, saved_out, log_shift, out_grad,
    )


def solution(mesh):
    return jax.shard_map(
        shards,
        mesh=mesh,
        in_specs=(
            P(("grp", "sp", "tp"), None),
            P(("grp", "sp", "tp"), None),
            P(),
            P(None, "tp"),
            P(),
            P(),
            P("tp", None),
            P(("grp", "sp"), "tp"),
            P("tp", ("grp", "sp")),
            P(("grp", "sp", "tp"), None),
        ),
        out_specs=(
            P(("grp", "sp", "tp"), None),
            P(("grp", "sp", "tp"), None),
            P(("grp", "sp"), "tp"),
        ),
        check_vma=False,
    )
```

time: 144 us -> 121 us (0.84)
  Pallas kernels: 131 us -> 116 us
  local copies, waits for them, and re-layouts: 11.2 us -> 4.01 us
    pallas_call x1, Pallas kernels: 131 us -> 116 us  [shards(): pl.pallas_call(functools.partial(kernel, (n, m, rows, srows, width)), out...]
    unnamed x23 -> x5, local copies, waits for them, and re-layouts: 11.2 us -> 4.01 us
where the time goes in v2:
time: 121 us
  Pallas kernels  116 us (96%)
  local copies, waits for them, and re-layouts  4.01 us (3%)
    pallas_call x1, Pallas kernels, shards(): pl.pallas_call(functools.partial(kernel, (n, m, rows, srows, width)), out...  116 us
    unnamed x5, local copies, waits for them, and re-layouts  4.01 us

profile of v2, /device:TPU:80, one launch (start us, length us, event | category | flops | bytes accessed | tf_op | source)
XLA Modules:
  0.0 120.7 jit_solution(679100303443071219)
XLA Ops:
  0.6 116.0 %shard_map.121 = (f32[8,2048]{1,0:T(8,128)}, f32[64,2048]{1,0:T(8,128)}, f32[128,128]{1,0:T(8,128)}) custom-call(bf16[8,2048]{1,0:T(8,128)(2,1)} %refs_0_.1, bf16[64,2048]{1,0:T(8,128)(2,1)} %refs_1_.1, f32[1,2048]{1,0:T(1,128)} %bitcast.1, bf16[2048,128]{1,0:T(8,128)(2,1)} %refs_3_.1, bf16[2048,256]{1,0:T(8,128)(2,1)} %refs_4_.1, ...), custom_call_target="tpu_custom_call" | custom-call | tf_op jit(solution)/shard_map/pallas_call | solution.py:542
  116.7 1.5 %copy.16 = f32[8,2048]{1,0:T(8,128)} copy(f32[8,2048]{1,0:T(8,128)} %get-tuple-element.6) | data formatting | bytes 131072
  118.1 0.0 copy-start
  118.1 1.9 %copy.17 = f32[64,2048]{1,0:T(8,128)} copy(f32[64,2048]{1,0:T(8,128)} %get-tuple-element.7) | data formatting | bytes 1048576
  120.0 0.0 copy-done
  120.0 0.6 copy.18
Async XLA Ops:
  118.1 1.9 %copy-start = (f32[128,128]{1,0:T(8,128)S(1)}, f32[128,128]{1,0:T(8,128)}, u32[]{:S(2)}) copy-start(f32[128,128]{1,0:T(8,128)} %get-tuple-element.8) | copy-start | bytes 196612
